TPU v7x, 32 devices: a whole 2x2x4 slice. The times are simulated.
32 devices in a mesh: sp: 16 (over z, y, x), tp: 2 (over core).
Axes of the slice: x: 2, y: 2, z: 4, core: 2. Of those that a mesh axis runs over, the one named last changes fastest.
Arguments:
- residual: bfloat16 [2048, 2048], P('sp'), may hold values from -6 to 6
- query_nope: bfloat16 [2048, 8, 128], P('sp', 'tp'), may hold values from -6 to 6
- query_rope: bfloat16 [2048, 8, 64], P('sp', 'tp'), may hold values from -64 to 64
- latent: bfloat16 [2048, 256], P('sp'), may hold values from -6 to 6
- rope_key: bfloat16 [2048, 64], P('sp'), may hold values from -64 to 64
- kv_gain: bfloat16 [256], replicated, may hold values from 0.099609375 to 1.8984375
- key_up: bfloat16 [256, 8, 128], replicated, may hold values from -0.375 to 0.375
- value_up: bfloat16 [256, 8, 128], replicated, may hold values from -0.375 to 0.375
- out_weight: bfloat16 [1024, 2048], P('tp'), may hold values from -0.1875 to 0.1875
- post_gain: bfloat16 [2048], replicated, may hold values from 0.099609375 to 1.8984375
- pre_gain: bfloat16 [2048], replicated, may hold values from 0.099609375 to 1.8984375
- ffn_gain: bfloat16 [2048], replicated, may hold values from 0.099609375 to 1.8984375
- up_value: bfloat16 [2048, 5632], P('sp', 'tp'), may hold values from -0.125 to 0.125
- up_gate: bfloat16 [2048, 5632], P('sp', 'tp'), may hold values from -0.125 to 0.125
- conv_value: bfloat16 [3, 5632], replicated, may hold values from -3.5 to 3.5
- conv_gate: bfloat16 [3, 5632], replicated, may hold values from -3.5 to 3.5
- down_weight: bfloat16 [5632, 2048], P('tp', 'sp'), may hold values from -0.078125 to 0.078125
Outputs:
- layer_out: bfloat16 [2048, 2048], P(('sp', 'tp'))
All inputs are finite; a program needn't handle non-finite values.
Results may differ from a plain program's by a relative error of at most 0.02.
Values may be sent and summed in bfloat16 or wider, within the bound.
No kernel may reach another device: no remote copies, remote signals or barrier semaphores. Data moves between devices by JAX's collectives and lax.ppermute only.
A program may use at most 128 MiB of HBM per device.

v0:
```python
import jax
import jax.numpy as jnp
from jax import lax
from jax.sharding import PartitionSpec as P

GRID = 64
epsilon = 1e-06
rope_base = 10000.0


def extended(x, sides, width):
    for axis, dim in sides:
        size, length = (lax.axis_size(axis), x.shape[dim])
        up = [(i, (i + 1) % size) for i in range(size - 1)]
        down = [(j, i) for i, j in up]
        last = lax.slice_in_dim(x, length - width, length, axis=dim)
        initial = lax.slice_in_dim(x, 0, width, axis=dim)
        before = lax.ppermute(last, axis, up)
        after = lax.ppermute(initial, axis, down)
        x = jnp.concatenate([before, x, after], axis=dim)
    return x


def rms_norm(values, gain):
    return (
        values
        * lax.rsqrt(jnp.mean(values * values, axis=-1, keepdims=True) + epsilon)
        * gain.astype(jnp.float32)
    )


def widened(values):
    return lax.optimization_barrier(values.astype(jnp.bfloat16)).astype(jnp.float32)


def rotate(values, positions):
    pair_count = values.shape[-1] // 4
    frequency = rope_base ** (-jnp.arange(pair_count, dtype=jnp.float32) / pair_count)
    grid_rows = (positions // GRID).astype(jnp.float32)
    grid_cols = (positions % GRID).astype(jnp.float32)
    angles = jnp.stack([grid_rows, grid_cols], axis=-1)[:, :, None] * frequency
    table_shape = (angles.shape[0],) + (1,) * (values.ndim - 2) + angles.shape[1:]
    cosine = jnp.cos(angles).reshape(table_shape)
    sine = jnp.sin(angles).reshape(table_shape)
    halves = values.reshape(values.shape[:-1] + (2, 2, pair_count))
    leading = halves[..., 0, :]
    trailing = halves[..., 1, :]
    turned = jnp.stack(
        [leading * cosine - trailing * sine, trailing * cosine + leading * sine], axis=-2
    )
    return turned.reshape(values.shape)


def body(
    residual,
    query_nope,
    query_rope,
    latent,
    rope_key,
    kv_gain,
    key_up,
    value_up,
    out_weight,
    post_gain,
    pre_gain,
    ffn_gain,
    up_value,
    up_gate,
    conv_value,
    conv_gate,
    down_weight,
):
    tok_rows = residual.shape[0]
    heads_dev = query_nope.shape[1]
    value_width = value_up.shape[2]
    tp_index = lax.axis_index("tp")
    positions = lax.axis_index("sp") * tok_rows + jnp.arange(tok_rows, dtype=jnp.int32)
    score_scale = (query_nope.shape[2] + query_rope.shape[2]) ** (-0.5)
    normed = rms_norm(latent.astype(jnp.float32), kv_gain).astype(jnp.bfloat16)
    key_turn = rotate(rope_key.astype(jnp.float32), positions).astype(jnp.bfloat16)
    query_turn = rotate(query_rope.astype(jnp.float32), positions).astype(jnp.bfloat16)
    key_local = lax.dynamic_slice_in_dim(key_up, tp_index * heads_dev, heads_dev, 1)
    value_local = lax.dynamic_slice_in_dim(value_up, tp_index * heads_dev, heads_dev, 1)
    pieces = (
        lax.all_gather(normed, "sp", axis=0, tiled=True),
        lax.all_gather(key_turn, "sp", axis=0, tiled=True),
    )
    keys_nope = jnp.einsum(
        "nc,chd->nhd", pieces[0], key_local, preferred_element_type=jnp.float32
    ).astype(jnp.bfloat16)
    values_part = jnp.einsum(
        "nc,chd->nhd", pieces[0], value_local, preferred_element_type=jnp.float32
    ).astype(jnp.bfloat16)
    row_max = jnp.full((heads_dev, tok_rows), -1e30, jnp.float32)
    scores = (
        jnp.einsum("qhd,khd->hqk", query_nope, keys_nope, preferred_element_type=jnp.float32)
        + jnp.einsum("qhd,kd->hqk", query_turn, pieces[1], preferred_element_type=jnp.float32)
    ) * score_scale
    new_max = jnp.maximum(row_max, jnp.max(scores, axis=-1))
    weights = jnp.exp(scores - new_max[:, :, None])
    totals = jnp.sum(weights, axis=-1)
    weighted = jnp.einsum(
        "hqk,khd->hqd",
        weights.astype(jnp.bfloat16),
        values_part,
        preferred_element_type=jnp.float32,
    )
    attended = (weighted / totals[:, :, None]).astype(jnp.bfloat16)
    attended = jnp.transpose(attended, (1, 0, 2)).reshape(tok_rows, heads_dev * value_width)
    row_share = tok_rows // lax.axis_size("tp")
    summed = lax.psum_scatter(
        jnp.dot(attended, out_weight, preferred_element_type=jnp.float32).astype(jnp.bfloat16),
        "tp",
        scatter_dimension=0,
        tiled=True,
    ).astype(jnp.float32)
    own_rows = lax.dynamic_slice_in_dim(residual, tp_index * row_share, row_share, 0).astype(
        jnp.float32
    )
    stream_wide = widened(own_rows + rms_norm(widened(summed), post_gain))
    inputs = lax.all_gather(
        rms_norm(stream_wide, pre_gain).astype(jnp.bfloat16), "tp", axis=0, tiled=True
    )
    ff_dev = up_value.shape[1]
    up_joined = jnp.concatenate([up_value, up_gate], axis=1)
    up_whole = lax.all_gather(up_joined, "sp", axis=0, tiled=True)
    up_pair = jnp.dot(inputs, up_whole, preferred_element_type=jnp.float32).astype(jnp.bfloat16)
    padded = extended(up_pair, (("sp", 0),), 1).astype(jnp.float32)
    channel_start = tp_index * ff_dev
    conv_taps = jnp.concatenate(
        [
            lax.dynamic_slice_in_dim(conv_value, channel_start, ff_dev, 1),
            lax.dynamic_slice_in_dim(conv_gate, channel_start, ff_dev, 1),
        ],
        axis=1,
    ).astype(jnp.float32)
    mixed_conv = (
        padded[:-2] * conv_taps[0] + padded[1:-1] * conv_taps[1] + padded[2:] * conv_taps[2]
    )
    hidden = (jax.nn.silu(mixed_conv[:, ff_dev:]) * mixed_conv[:, :ff_dev]).astype(jnp.bfloat16)
    down_whole = lax.all_gather(down_weight, "sp", axis=1, tiled=True)
    down_terms = jnp.dot(hidden, down_whole, preferred_element_type=jnp.float32)
    reduced = lax.psum_scatter(
        down_terms.astype(jnp.bfloat16), "tp", scatter_dimension=0, tiled=True
    ).astype(jnp.float32)
    return (stream_wide + rms_norm(widened(reduced), ffn_gain)).astype(jnp.bfloat16)


def solution(mesh):
    placed = (
        P("sp", None),
        P("sp", "tp", None),
        P("sp", "tp", None),
        P("sp", None),
        P("sp", None),
        P(),
        P(),
        P(),
        P("tp", None),
        P(),
        P(),
        P(),
        P("sp", "tp"),
        P("sp", "tp"),
        P(),
        P(),
        P("tp", "sp"),
    )
    return jax.shard_map(
        body, mesh=mesh, in_specs=placed, out_specs=P(("sp", "tp"), None), check_vma=False
    )
```

profile of v0, /device:TPU:0, one launch (start us, length us, event | category | flops | bytes accessed | tf_op | source)
XLA Modules:
  0.0 553.0 jit_solution(2200279591683789855)
XLA Ops:
  6.5 0.0 copy-start
  6.5 0.0 all-gather.4.cloned.1.call-start
  6.5 1.1 fusion.40
  7.6 0.7 convert_element_type.108
  8.3 1.6 fusion.42
  9.9 0.0 all-gather.4.cloned.1.call-update
  9.9 0.0 reduce-scatter.3.cloned.1.call-start
  9.9 0.9 convert.19
  10.8 0.7 convert.18
  11.6 0.1 fusion.51
  11.7 0.1 multiply_cosine_fusion
  11.9 44.1 %all_gather.16 = bf16[2048,64]{0,1:T(8,128)(2,1)S(1)} all-gather(bf16[128,64]{0,1:T(8,128)(2,1)S(1)} %bitcast.41), channel_id=1, replica_groups=mesh['sp'=16,'tp'=2] {'sp'}, dimensions={0}, use_global_device_ids=true | all-gather | bytes 278528 | tf_op jit(solution)/shard_map/all_gather | solution.py:86
  56.0 1.5 constant_dynamic-slice_fusion.2
  57.5 10.8 %all-gather.4.cloned.1.call-done = bf16[2048,256]{1,0:T(8,128)(2,1)} async-done(((bf16[128,256]{1,0:T(8,128)(2,1)}), bf16[2048,256]{1,0:T(8,128)(2,1)}) %all-gather.4.cloned.1.call-update) | async-done | bytes 1048592 | tf_op jit(solution)/shard_map/all_gather | solution.py:85
  68.3 4.4 fusion.8
  72.7 2.9 fusion.58
  75.7 0.0 copy-start.1
  75.7 0.0 copy-start.2
  75.7 1.9 copy-done.1
  77.6 0.6 fusion.1
  78.2 0.0 copy-done.2
  78.2 4.3 fusion.16
  82.5 0.0 copy-start.3
  82.5 0.0 copy-start.4
  82.5 0.0 copy-done
  82.5 2.3 convolution_convert_fusion.4
  84.7 0.0 copy-start.5
  84.8 0.0 copy-start.6
  84.8 0.0 reduce-scatter.3.cloned.1.call-update
  84.8 0.0 all-gather.6.cloned.1.call-start
  84.8 0.0 copy-done.3
  84.8 0.0 copy-done.4
  84.8 1.2 pad_maximum_fusion
  86.0 0.0 all-gather.6.cloned.1.call-update
  86.1 0.0 all-gather.8.cloned.1.call-start
  86.1 0.5 all-gather.8.cloned.1.call-update
  86.7 0.0 reduce-scatter.5.cloned.1.call-start
  86.7 0.0 copy-done.5
  86.7 0.0 copy-done.6
  86.7 0.8 constant_dynamic-slice_fusion
  87.5 4.2 reduce-scatter.3.cloned.1.call-done
  91.7 1.1 fusion.25
  92.8 1.2 fusion.28
  94.0 0.2 fusion.31
  94.2 0.1 fusion.33
  94.3 2.2 all_gather.17
  96.5 249.5 %all-gather.6.cloned.1.call-done = bf16[2048,5632]{1,0:T(8,128)(2,1)} async-done(((bf16[128,5632]{1,0:T(8,128)(2,1)}), bf16[2048,5632]{1,0:T(8,128)(2,1)}) %all-gather.6.cloned.1.call-update) | async-done | bytes 23068688 | tf_op jit(solution)/shard_map/all_gather | solution.py:126
  346.1 10.7 %convolution_convert_fusion = bf16[128,5632]{1,0:T(8,128)(2,1)S(1)} fusion(bf16[128,2048]{1,0:T(8,128)(2,1)S(1)} %all_gather.17, bf16[2048,5632]{1,0:T(8,128)(2,1)} %all-gather.6.cloned.1.call-done), kind=kOutput, calls=%fused_computation | convolution fusion | flops 2953510912 | bytes 25034752 | tf_op jit(solution)/shard_map/dot_general | solution.py:127
  356.8 3.4 collective-permute-start
  360.2 1.5 collective-permute-start.1
  361.7 0.2 convert_reduce_fusion.1
  361.9 0.2 collective-permute-done
  362.1 4.4 collective-permute-done.1
  366.5 0.4 maximum_convert_fusion
  366.9 2.4 fusion.3
  369.4 0.0 copy-start.7
  369.4 160.2 %all-gather.8.cloned.1.call-done = bf16[2816,2048]{1,0:T(8,128)(2,1)} async-done(((bf16[2816,128]{1,0:T(8,128)(2,1)}), bf16[2816,2048]{1,0:T(8,128)(2,1)}) %all-gather.8.cloned.1.call-update) | async-done | bytes 11534352 | tf_op jit(solution)/shard_map/all_gather | solution.py:141
  529.5 7.7 %convolution_convert_fusion.3 = bf16[128,2048]{1,0:T(8,128)(2,1)} fusion(bf16[2816,2048]{1,0:T(8,128)(2,1)} %all-gather.8.cloned.1.call-done, f32[128,5632]{1,0:T(8,128)} %fusion.3), kind=kOutput, calls=%fused_computation.13 | convolution fusion | flops 1478819840 | bytes 14942208 | tf_op jit(solution)/shard_map/dot_general | solution.py:142
  537.2 0.0 reduce-scatter.5.cloned.1.call-update
  537.3 0.0 copy-done.7
  537.3 6.2 %reduce-scatter.5.cloned.1.call-done = bf16[64,2048]{1,0:T(8,128)(2,1)} async-done(((bf16[128,2048]{1,0:T(8,128)(2,1)}), bf16[64,2048]{1,0:T(8,128)(2,1)}) %reduce-scatter.5.cloned.1.call-update) | async-done | bytes 262160 | tf_op jit(solution)/shard_map/reduce_scatter | solution.py:143
  543.5 1.1 fusion.29
  544.6 1.8 fusion.34
  (15 shorter events, 0.2 us)
Async XLA Ops:
  6.5 75.9 %copy-start = (bf16[512,2048]{1,0:T(8,128)(2,1)S(1)}, bf16[512,2048]{1,0:T(8,128)(2,1)}, u32[]{:S(2)}) copy-start(bf16[512,2048]{1,0:T(8,128)(2,1)} %param.25) | copy-start | bytes 6291460
  6.5 61.8 %all-gather.4.cloned.1.call-start = ((), (), s32[]{:S(2)}) async-start(), calls=%async_computation.2 | async-start | bytes 1114112 | tf_op jit(solution)/shard_map/all_gather | solution.py:85
  9.9 81.8 %reduce-scatter.3.cloned.1.call-start = ((), (), s32[]{:S(2)}) async-start(), calls=%async_computation.3 | async-start | bytes 786432 | tf_op jit(solution)/shard_map/reduce_scatter | solution.py:111
  75.7 1.9 copy-start.1
  75.7 2.5 copy-start.2
  82.5 2.4 copy-start.3
  82.5 2.4 copy-start.4
  84.7 2.0 copy-start.5
  84.8 2.0 copy-start.6
  84.8 261.3 %all-gather.6.cloned.1.call-start = ((), (), s32[]{:S(2)}) async-start(), calls=%async_computation.4 | async-start | bytes 24510464 | tf_op jit(solution)/shard_map/all_gather | solution.py:126
  86.1 443.5 %all-gather.8.cloned.1.call-start = ((), (), s32[]{:S(2)}) async-start(), calls=%async_computation.5 | async-start | bytes 12255232 | tf_op jit(solution)/shard_map/all_gather | solution.py:141
  86.7 456.9 %reduce-scatter.5.cloned.1.call-start = ((), (), s32[]{:S(2)}) async-start(), calls=%async_computation.6 | async-start | bytes 786432 | tf_op jit(solution)/shard_map/reduce_scatter | solution.py:143
  356.8 5.3 collective-permute-start
  360.2 6.3 %collective-permute-start.1 = (bf16[1,5632]{1,0:T(2,128)(2,1)S(1)}, bf16[1,5632]{1,0:T(2,128)(2,1)S(1)}, u32[]{:S(2)}, u32[]{:S(2)}) collective-permute-start(bf16[1,5632]{1,0:T(2,128)(2,1)S(1)} %get-tuple-element.9), channel_id=1, source_target_pairs={{2,0},{4,2},{6,4},{8,6},{10,8},{12,10},{14,12},{16,14},{18,16},{20... | collective-permute-start | bytes 33800 | tf_op jit(solution)/shard_map/ppermute | solution.py:19
  369.4 167.9 %copy-start.7 = (bf16[2048]{0:T(1024)(128)(2,1)S(1)}, bf16[2048]{0:T(1024)(128)(2,1)}, u32[]{:S(2)}) copy-start(bf16[2048]{0:T(1024)(128)(2,1)} %param.28) | copy-start | bytes 12292
Sparse Core Ops, SparseCore 0:
  10.1 58.1 all-gather.3
  84.9 6.7 reduce-scatter.2
  94.4 251.6 all-gather.5
  348.6 180.8 all-gather.7
  537.4 6.0 reduce-scatter.4
where the time goes:
time: 554 us; the launch traced here: 553 us
  waiting for transfers between devices  436 us (79%)
  blocking collectives  46.3 us (8%)
  matrix products  32.3 us (6%)
  other arithmetic  15.6 us (3%)
  between operations  13.4 us (2%)
    all_gather x1, waiting for transfers between devices, body(): up_whole = lax.all_gather(up_joined, 'sp', axis=0, tiled=True)  250 us
    all_gather x1, waiting for transfers between devices, body(): down_whole = lax.all_gather(down_weight, 'sp', axis=1, tiled=True)  160 us
    all_gather x1, blocking collectives, body(): lax.all_gather(key_turn, 'sp', axis=0, tiled=True)  44.1 us
  transfers between devices with their start and end apart: 7, of which 7 were waited for; matrix products, arithmetic and copies ran while one was open for 4% of the time, Pallas kernels for 0%

commit v1 on v0

--- a/solution.py
+++ b/solution.py
@@ -1,3 +1,4 @@
+import functools
 import jax
 import jax.numpy as jnp
 from jax import lax
@@ -6,6 +7,22 @@
 GRID = 64
 epsilon = 1e-06
 rope_base = 10000.0
+
+
+def time_the_pools(x_part, mesh_name, row_dim):
+    fan = jax.lax.axis_size(mesh_name)
+    x_now = sorted(((dev_i, (dev_i + 1) % fan) for dev_i in range(fan)))
+    big = x_part
+    runs = [big]
+    for h in range(1, fan):
+        big = jax.lax.ppermute(big, axis_name=mesh_name, perm=x_now)
+        runs.insert(0, big)
+    d_next = jnp.concatenate(runs, row_dim)
+    answer = jax.lax.axis_index(mesh_name) + 1
+    return jnp.roll(d_next, answer * x_part.shape[row_dim], row_dim)
+
+
+begin_skins = functools.partial(time_the_pools, mesh_name="sp", row_dim=0)
 
 
 def extended(x, sides, width):
@@ -123,7 +140,7 @@
     )
     ff_dev = up_value.shape[1]
     up_joined = jnp.concatenate([up_value, up_gate], axis=1)
-    up_whole = lax.all_gather(up_joined, "sp", axis=0, tiled=True)
+    up_whole = begin_skins(up_joined)
     up_pair = jnp.dot(inputs, up_whole, preferred_element_type=jnp.float32).astype(jnp.bfloat16)
     padded = extended(up_pair, (("sp", 0),), 1).astype(jnp.float32)
     channel_start = tp_index * ff_dev

time: 554 us -> 748 us (1.35)
  waiting for transfers between devices: 436 us -> 547 us
  local copies, waits for them, and re-layouts: 4.22 us -> 65.7 us
  blocking collectives: 46.3 us -> 58.6 us
    ppermute x0 -> x15, waiting for transfers between devices: none -> 446 us  [time_the_pools(): big = jax.lax.ppermute(big, axis_name=mesh_name, perm=x_now)]
    all_gather x1 -> x0, waiting for transfers between devices: 250 us -> none  [body(): up_whole = lax.all_gather(up_joined, 'sp', axis=0, tiled=True)]
    all_gather x1, waiting for transfers between devices: 160 us -> 90 us  [body(): down_whole = lax.all_gather(down_weight, 'sp', axis=1, tiled=True)]
    unnamed x16 -> x89, local copies, waits for them, and re-layouts: 1.93 us -> 61.6 us
    all_gather x1, blocking collectives: 44.1 us -> 56.2 us  [body(): lax.all_gather(key_turn, 'sp', axis=0, tiled=True)]
    all_gather x1, waiting for transfers between devices: 10.8 us -> 0.19 us  [body(): lax.all_gather(normed, 'sp', axis=0, tiled=True)]
    ppermute x0 -> x15, starting transfers between devices: none -> 7.64 us  [time_the_pools(): big = jax.lax.ppermute(big, axis_name=mesh_name, perm=x_now)]
  transfers between devices with their start and end apart: 7 -> 21, of which waited for: 7 -> 19; matrix products, arithmetic and copies ran while one was open for 4% -> 13% of each run, Pallas kernels for 0% -> 0%
where the time goes in v1:
time: 748 us; the launch traced here: 747 us
  waiting for transfers between devices  547 us (73%)
  local copies, waits for them, and re-layouts  65.7 us (9%)
  blocking collectives  58.6 us (8%)
  matrix products  33 us (4%)
  other arithmetic  19.3 us (3%)
  between operations  13.5 us (2%)
  starting transfers between devices  10.4 us (1%)
    ppermute x15, waiting for transfers between devices, time_the_pools(): big = jax.lax.ppermute(big, axis_name=mesh_name, perm=x_now)  446 us
    all_gather x1, waiting for transfers between devices, body(): down_whole = lax.all_gather(down_weight, 'sp', axis=1, tiled=True)  90 us
    unnamed x89, local copies, waits for them, and re-layouts  61.6 us
    all_gather x1, blocking collectives, body(): lax.all_gather(key_turn, 'sp', axis=0, tiled=True)  56.2 us
  transfers between devices with their start and end apart: 21, of which 19 were waited for; matrix products, arithmetic and copies ran while one was open for 13% of the time, Pallas kernels for 0%

profile of v1, /device:TPU:0, one launch (start us, length us, event | category | flops | bytes accessed | tf_op | source)
XLA Modules:
  0.0 747.0 jit_solution(4209762442526547862)
XLA Ops:
  6.5 1.6 pad_maximum_fusion
  8.1 3.0 collective-permute-start
  11.1 35.6 %collective-permute-done = bf16[128,5632]{1,0:T(8,128)(2,1)S(1)} collective-permute-done((bf16[128,5632]{1,0:T(8,128)(2,1)S(1)}, bf16[128,5632]{1,0:T(8,128)(2,1)S(1)}, u32[]{:S(2)}, u32[]{:S(2)}) %collective-permute-start) | collective-permute-done | bytes 1441824 | tf_op jit(solution)/shard_map/ppermute | solution.py:18
  46.7 36.3 %collective-permute-done.1 = bf16[128,5632]{1,0:T(8,128)(2,1)S(1)} collective-permute-done((bf16[128,5632]{1,0:T(8,128)(2,1)S(1)}, bf16[128,5632]{1,0:T(8,128)(2,1)S(1)}, u32[]{:S(2)}, u32[]{:S(2)}) %collective-permute-start.1) | collective-permute-done | bytes 1441824 | tf_op jit(solution)/shard_map/ppermute | solution.py:18
  84.2 35.5 %collective-permute-done.2 = bf16[128,5632]{1,0:T(8,128)(2,1)S(1)} collective-permute-done((bf16[128,5632]{1,0:T(8,128)(2,1)S(1)}, bf16[128,5632]{1,0:T(8,128)(2,1)S(1)}, u32[]{:S(2)}, u32[]{:S(2)}) %collective-permute-start.2) | collective-permute-done | bytes 1441824 | tf_op jit(solution)/shard_map/ppermute | solution.py:18
  120.8 34.6 %collective-permute-done.3 = bf16[128,5632]{1,0:T(8,128)(2,1)S(1)} collective-permute-done((bf16[128,5632]{1,0:T(8,128)(2,1)S(1)}, bf16[128,5632]{1,0:T(8,128)(2,1)S(1)}, u32[]{:S(2)}, u32[]{:S(2)}) %collective-permute-start.3) | collective-permute-done | bytes 1441824 | tf_op jit(solution)/shard_map/ppermute | solution.py:18
  156.5 33.8 %collective-permute-done.4 = bf16[128,5632]{1,0:T(8,128)(2,1)S(1)} collective-permute-done((bf16[128,5632]{1,0:T(8,128)(2,1)S(1)}, bf16[128,5632]{1,0:T(8,128)(2,1)S(1)}, u32[]{:S(2)}, u32[]{:S(2)}) %collective-permute-start.4) | collective-permute-done | bytes 1441824 | tf_op jit(solution)/shard_map/ppermute | solution.py:18
  191.5 32.9 %collective-permute-done.5 = bf16[128,5632]{1,0:T(8,128)(2,1)S(1)} collective-permute-done((bf16[128,5632]{1,0:T(8,128)(2,1)S(1)}, bf16[128,5632]{1,0:T(8,128)(2,1)S(1)}, u32[]{:S(2)}, u32[]{:S(2)}) %collective-permute-start.5) | collective-permute-done | bytes 1441824 | tf_op jit(solution)/shard_map/ppermute | solution.py:18
  225.5 32.1 %collective-permute-done.6 = bf16[128,5632]{1,0:T(8,128)(2,1)S(1)} collective-permute-done((bf16[128,5632]{1,0:T(8,128)(2,1)S(1)}, bf16[128,5632]{1,0:T(8,128)(2,1)S(1)}, u32[]{:S(2)}, u32[]{:S(2)}) %collective-permute-start.6) | collective-permute-done | bytes 1441824 | tf_op jit(solution)/shard_map/ppermute | solution.py:18
  258.7 31.2 %collective-permute-done.7 = bf16[128,5632]{1,0:T(8,128)(2,1)S(1)} collective-permute-done((bf16[128,5632]{1,0:T(8,128)(2,1)S(1)}, bf16[128,5632]{1,0:T(8,128)(2,1)S(1)}, u32[]{:S(2)}, u32[]{:S(2)}) %collective-permute-start.7) | collective-permute-done | bytes 1441824 | tf_op jit(solution)/shard_map/ppermute | solution.py:18
  291.0 30.6 %collective-permute-done.8 = bf16[128,5632]{1,0:T(8,128)(2,1)S(1)} collective-permute-done((bf16[128,5632]{1,0:T(8,128)(2,1)S(1)}, bf16[128,5632]{1,0:T(8,128)(2,1)S(1)}, u32[]{:S(2)}, u32[]{:S(2)}) %collective-permute-start.8) | collective-permute-done | bytes 1441824 | tf_op jit(solution)/shard_map/ppermute | solution.py:18
  322.7 31.5 %collective-permute-done.9 = bf16[128,5632]{1,0:T(8,128)(2,1)} collective-permute-done((bf16[128,5632]{1,0:T(8,128)(2,1)S(1)}, bf16[128,5632]{1,0:T(8,128)(2,1)}, u32[]{:S(2)}, u32[]{:S(2)}) %collective-permute-start.9) | collective-permute-done | bytes 1441824 | tf_op jit(solution)/shard_map/ppermute | solution.py:18
  355.9 1.5 fusion.47
  357.5 1.5 convert.19
  359.0 1.3 convert.18
  360.4 28.2 %collective-permute-done.10 = bf16[128,5632]{1,0:T(8,128)(2,1)} collective-permute-done((bf16[128,5632]{1,0:T(8,128)(2,1)}, bf16[128,5632]{1,0:T(8,128)(2,1)}, u32[]{:S(2)}, u32[]{:S(2)}) %collective-permute-start.10) | collective-permute-done | bytes 1441824 | tf_op jit(solution)/shard_map/ppermute | solution.py:18
  391.2 56.2 %all_gather.13 = bf16[2048,64]{0,1:T(8,128)(2,1)} all-gather(bf16[128,64]{0,1:T(8,128)(2,1)S(1)} %bitcast.40), channel_id=1, replica_groups=mesh['sp'=16,'tp'=2] {'sp'}, dimensions={0}, use_global_device_ids=true | all-gather | bytes 278528 | tf_op jit(solution)/shard_map/all_gather | solution.py:103
  447.4 2.3 constant_dynamic-slice_fusion.2
  449.9 4.5 fusion.13
  454.4 2.2 collective-permute-start.12
  456.6 3.1 fusion.64
  459.7 1.9 copy-done.2
  462.2 4.7 fusion.21
  466.9 2.2 convolution_convert_fusion.3
  469.2 20.8 %collective-permute-done.12 = bf16[128,5632]{1,0:T(8,128)(2,1)} collective-permute-done((bf16[128,5632]{1,0:T(8,128)(2,1)}, bf16[128,5632]{1,0:T(8,128)(2,1)}, u32[]{:S(2)}, u32[]{:S(2)}) %collective-permute-start.12) | collective-permute-done | bytes 1441824 | tf_op jit(solution)/shard_map/ppermute | solution.py:18
  492.1 35.2 %collective-permute-done.13 = bf16[128,5632]{1,0:T(8,128)(2,1)S(1)} collective-permute-done((bf16[128,5632]{1,0:T(8,128)(2,1)}, bf16[128,5632]{1,0:T(8,128)(2,1)S(1)}, u32[]{:S(2)}, u32[]{:S(2)}) %collective-permute-start.13) | collective-permute-done | bytes 1441824 | tf_op jit(solution)/shard_map/ppermute | solution.py:18
  527.3 2.4 collective-permute-start.14
  529.7 1.2 fusion.33
  531.3 2.4 all_gather.14
  533.6 27.1 %collective-permute-done.14 = bf16[128,5632]{1,0:T(8,128)(2,1)S(1)} collective-permute-done((bf16[128,5632]{1,0:T(8,128)(2,1)S(1)}, bf16[128,5632]{1,0:T(8,128)(2,1)S(1)}, u32[]{:S(2)}, u32[]{:S(2)}) %collective-permute-start.14) | collective-permute-done | bytes 1441824 | tf_op jit(solution)/shard_map/ppermute | solution.py:18
  560.7 1.2 constant_dynamic-update-slice_fusion.31
  562.0 1.2 constant_dynamic-update-slice_fusion.30
  563.1 2.6 constant_dynamic-update-slice_fusion.29
  565.7 2.7 constant_dynamic-update-slice_fusion.28
  568.4 2.7 constant_dynamic-update-slice_fusion.27
  571.2 2.8 constant_dynamic-update-slice_fusion.26
  574.0 1.2 constant_dynamic-update-slice_fusion.25
  575.2 1.2 constant_dynamic-update-slice_fusion.24
  576.4 1.3 constant_dynamic-update-slice_fusion.23
  578.8 1.2 constant_dynamic-update-slice_fusion.21
  580.1 1.2 constant_dynamic-update-slice_fusion.20
  581.3 1.2 constant_dynamic-update-slice_fusion.19
  582.5 1.2 constant_dynamic-update-slice_fusion.18
  586.8 1.2 constant_dynamic-update-slice_fusion.15
  588.0 1.3 constant_dynamic-update-slice_fusion.14
  589.3 2.6 constant_dynamic-update-slice_fusion.13
  591.9 2.6 constant_dynamic-update-slice_fusion.12
  594.5 2.6 constant_dynamic-update-slice_fusion.11
  597.1 2.6 constant_dynamic-update-slice_fusion.10
  599.7 1.2 constant_dynamic-update-slice_fusion.9
  600.8 1.2 constant_dynamic-update-slice_fusion.8
  603.2 1.2 constant_dynamic-update-slice_fusion.6
  605.7 1.2 constant_dynamic-update-slice_fusion.4
  606.9 1.3 constant_dynamic-update-slice_fusion.3
  608.1 1.2 constant_dynamic-update-slice_fusion.2
  612.4 10.7 %fusion.2 = bf16[128,5632]{1,0:T(8,128)(2,1)S(1)} fusion(bf16[128,2048]{1,0:T(8,128)(2,1)S(1)} %all_gather.14, bf16[4096,5632]{1,0:T(8,128)(2,1)} %constant_dynamic-update-slice_fusion.32, s32[]{:T(128)S(6)} %select_n.57), kind=kOutput, calls=%fused_computation.2 | convolution fusion | flops 2953510912 | bytes 25034756 | tf_op jit(solution)/shard_map/dot_general | solution.py:144
  623.2 1.3 collective-permute-start.15
  624.5 1.3 collective-permute-start.16
  626.2 4.6 collective-permute-done.16
  631.2 2.4 fusion.8
  633.6 90.0 %all-gather.5.cloned.1.call-done = bf16[2816,2048]{1,0:T(8,128)(2,1)} async-done(((bf16[2816,128]{1,0:T(8,128)(2,1)}), bf16[2816,2048]{1,0:T(8,128)(2,1)}) %all-gather.5.cloned.1.call-update) | async-done | bytes 11534352 | tf_op jit(solution)/shard_map/all_gather | solution.py:158
  723.6 7.8 %convolution_convert_fusion.2 = bf16[128,2048]{1,0:T(8,128)(2,1)} fusion(bf16[2816,2048]{1,0:T(8,128)(2,1)} %all-gather.5.cloned.1.call-done, f32[128,5632]{1,0:T(8,128)} %fusion.8), kind=kOutput, calls=%fused_computation.15 | convolution fusion | flops 1478819840 | bytes 14942208 | tf_op jit(solution)/shard_map/dot_general | solution.py:159
  731.5 6.0 reduce-scatter.5.cloned.1.call-done
  738.6 1.8 fusion.39
  (115 shorter events, 28.1 us)
Async XLA Ops:
  6.5 460.4 %copy-start = (bf16[512,2048]{1,0:T(8,128)(2,1)S(1)}, bf16[512,2048]{1,0:T(8,128)(2,1)}, u32[]{:S(2)}) copy-start(bf16[512,2048]{1,0:T(8,128)(2,1)} %param.25) | copy-start | bytes 6291460
  6.5 443.3 %all-gather.3.cloned.1.call-start = ((), (), s32[]{:S(2)}) async-start(), calls=%async_computation.2 | async-start | bytes 1114112 | tf_op jit(solution)/shard_map/all_gather | solution.py:102
  8.1 38.6 %collective-permute-start = (bf16[128,5632]{1,0:T(8,128)(2,1)S(1)}, bf16[128,5632]{1,0:T(8,128)(2,1)S(1)}, u32[]{:S(2)}, u32[]{:S(2)}) collective-permute-start(bf16[128,5632]{1,0:T(8,128)(2,1)S(1)} %pad_maximum_fusion), channel_id=1, source_target_pairs={{0,2},{2,4},{4,6},{6,8},{8,10},{10,12},{12,14},{14,16},{16,18},{18... | collective-permute-start | bytes 4325384 | tf_op jit(solution)/shard_map/ppermute | solution.py:18
  46.7 36.3 %collective-permute-start.1 = (bf16[128,5632]{1,0:T(8,128)(2,1)S(1)}, bf16[128,5632]{1,0:T(8,128)(2,1)S(1)}, u32[]{:S(2)}, u32[]{:S(2)}) collective-permute-start(bf16[128,5632]{1,0:T(8,128)(2,1)S(1)} %collective-permute-done), channel_id=1, source_target_pairs={{0,2},{2,4},{4,6},{6,8},{8,10},{10,12},{12,14},{14,16},{16,18},{18... | collective-permute-start | bytes 4325384 | tf_op jit(solution)/shard_map/ppermute | solution.py:18
  83.1 1.1 copy-start.5
  84.2 35.5 %collective-permute-start.2 = (bf16[128,5632]{1,0:T(8,128)(2,1)S(1)}, bf16[128,5632]{1,0:T(8,128)(2,1)S(1)}, u32[]{:S(2)}, u32[]{:S(2)}) collective-permute-start(bf16[128,5632]{1,0:T(8,128)(2,1)S(1)} %collective-permute-done.1), channel_id=1, source_target_pairs={{0,2},{2,4},{4,6},{6,8},{8,10},{10,12},{12,14},{14,16},{16,18},{18... | collective-permute-start | bytes 4325384 | tf_op jit(solution)/shard_map/ppermute | solution.py:18
  119.7 1.1 copy-start.7
  120.8 34.6 %collective-permute-start.3 = (bf16[128,5632]{1,0:T(8,128)(2,1)S(1)}, bf16[128,5632]{1,0:T(8,128)(2,1)S(1)}, u32[]{:S(2)}, u32[]{:S(2)}) collective-permute-start(bf16[128,5632]{1,0:T(8,128)(2,1)S(1)} %collective-permute-done.2), channel_id=1, source_target_pairs={{0,2},{2,4},{4,6},{6,8},{8,10},{10,12},{12,14},{14,16},{16,18},{18... | collective-permute-start | bytes 4325384 | tf_op jit(solution)/shard_map/ppermute | solution.py:18
  155.4 1.1 copy-start.9
  156.5 33.8 %collective-permute-start.4 = (bf16[128,5632]{1,0:T(8,128)(2,1)S(1)}, bf16[128,5632]{1,0:T(8,128)(2,1)S(1)}, u32[]{:S(2)}, u32[]{:S(2)}) collective-permute-start(bf16[128,5632]{1,0:T(8,128)(2,1)S(1)} %collective-permute-done.3), channel_id=1, source_target_pairs={{0,2},{2,4},{4,6},{6,8},{8,10},{10,12},{12,14},{14,16},{16,18},{18... | collective-permute-start | bytes 4325384 | tf_op jit(solution)/shard_map/ppermute | solution.py:18
  190.3 1.2 copy-start.11
  191.5 32.9 %collective-permute-start.5 = (bf16[128,5632]{1,0:T(8,128)(2,1)S(1)}, bf16[128,5632]{1,0:T(8,128)(2,1)S(1)}, u32[]{:S(2)}, u32[]{:S(2)}) collective-permute-start(bf16[128,5632]{1,0:T(8,128)(2,1)S(1)} %collective-permute-done.4), channel_id=1, source_target_pairs={{0,2},{2,4},{4,6},{6,8},{8,10},{10,12},{12,14},{14,16},{16,18},{18... | collective-permute-start | bytes 4325384 | tf_op jit(solution)/shard_map/ppermute | solution.py:18
  224.4 1.1 copy-start.13
  225.5 32.1 %collective-permute-start.6 = (bf16[128,5632]{1,0:T(8,128)(2,1)S(1)}, bf16[128,5632]{1,0:T(8,128)(2,1)S(1)}, u32[]{:S(2)}, u32[]{:S(2)}) collective-permute-start(bf16[128,5632]{1,0:T(8,128)(2,1)S(1)} %collective-permute-done.5), channel_id=1, source_target_pairs={{0,2},{2,4},{4,6},{6,8},{8,10},{10,12},{12,14},{14,16},{16,18},{18... | collective-permute-start | bytes 4325384 | tf_op jit(solution)/shard_map/ppermute | solution.py:18
  257.6 1.1 copy-start.15
  258.7 31.2 %collective-permute-start.7 = (bf16[128,5632]{1,0:T(8,128)(2,1)S(1)}, bf16[128,5632]{1,0:T(8,128)(2,1)S(1)}, u32[]{:S(2)}, u32[]{:S(2)}) collective-permute-start(bf16[128,5632]{1,0:T(8,128)(2,1)S(1)} %collective-permute-done.6), channel_id=1, source_target_pairs={{0,2},{2,4},{4,6},{6,8},{8,10},{10,12},{12,14},{14,16},{16,18},{18... | collective-permute-start | bytes 4325384 | tf_op jit(solution)/shard_map/ppermute | solution.py:18
  289.9 1.1 copy-start.17
  291.0 30.6 %collective-permute-start.8 = (bf16[128,5632]{1,0:T(8,128)(2,1)S(1)}, bf16[128,5632]{1,0:T(8,128)(2,1)S(1)}, u32[]{:S(2)}, u32[]{:S(2)}) collective-permute-start(bf16[128,5632]{1,0:T(8,128)(2,1)S(1)} %collective-permute-done.7), channel_id=1, source_target_pairs={{0,2},{2,4},{4,6},{6,8},{8,10},{10,12},{12,14},{14,16},{16,18},{18... | collective-permute-start | bytes 4325384 | tf_op jit(solution)/shard_map/ppermute | solution.py:18
  321.6 1.2 copy-start.19
  322.7 31.5 %collective-permute-start.9 = (bf16[128,5632]{1,0:T(8,128)(2,1)S(1)}, bf16[128,5632]{1,0:T(8,128)(2,1)}, u32[]{:S(2)}, u32[]{:S(2)}) collective-permute-start(bf16[128,5632]{1,0:T(8,128)(2,1)S(1)} %collective-permute-done.8), channel_id=1, source_target_pairs={{0,2},{2,4},{4,6},{6,8},{8,10},{10,12},{12,14},{14,16},{16,18},{18... | collective-permute-start | bytes 4325384 | tf_op jit(solution)/shard_map/ppermute | solution.py:18
  354.3 34.3 %collective-permute-start.10 = (bf16[128,5632]{1,0:T(8,128)(2,1)}, bf16[128,5632]{1,0:T(8,128)(2,1)}, u32[]{:S(2)}, u32[]{:S(2)}) collective-permute-start(bf16[128,5632]{1,0:T(8,128)(2,1)} %collective-permute-done.9), channel_id=1, source_target_pairs={{0,2},{2,4},{4,6},{6,8},{8,10},{10,12},{12,14},{14,16},{16,18},{18... | collective-permute-start | bytes 4325384 | tf_op jit(solution)/shard_map/ppermute | solution.py:18
  357.5 133.5 %reduce-scatter.3.cloned.1.call-start = ((), (), s32[]{:S(2)}) async-start(), calls=%async_computation.3 | async-start | bytes 786432 | tf_op jit(solution)/shard_map/reduce_scatter | solution.py:128
  388.6 65.8 %collective-permute-start.11 = (bf16[128,5632]{1,0:T(8,128)(2,1)}, bf16[128,5632]{1,0:T(8,128)(2,1)}, u32[]{:S(2)}, u32[]{:S(2)}) collective-permute-start(bf16[128,5632]{1,0:T(8,128)(2,1)} %collective-permute-done.10), channel_id=1, source_target_pairs={{0,2},{2,4},{4,6},{6,8},{8,10},{10,12},{12,14},{14,16},{16,18},{18... | collective-permute-start | bytes 4325384 | tf_op jit(solution)/shard_map/ppermute | solution.py:18
  454.4 35.6 %collective-permute-start.12 = (bf16[128,5632]{1,0:T(8,128)(2,1)}, bf16[128,5632]{1,0:T(8,128)(2,1)}, u32[]{:S(2)}, u32[]{:S(2)}) collective-permute-start(bf16[128,5632]{1,0:T(8,128)(2,1)} %collective-permute-done.11), channel_id=1, source_target_pairs={{0,2},{2,4},{4,6},{6,8},{8,10},{10,12},{12,14},{14,16},{16,18},{18... | collective-permute-start | bytes 4325384 | tf_op jit(solution)/shard_map/ppermute | solution.py:18
  459.7 2.0 copy-start.2
  462.2 27.9 %copy-start.25 = (bf16[2048]{0:T(1024)(128)(2,1)S(1)}, bf16[2048]{0:T(1024)(128)(2,1)}, u32[]{:S(2)}) copy-start(bf16[2048]{0:T(1024)(128)(2,1)} %param.26) | copy-start | bytes 12292
  462.2 27.9 %copy-start.26 = (bf16[2048]{0:T(1024)(128)(2,1)S(1)}, bf16[2048]{0:T(1024)(128)(2,1)}, u32[]{:S(2)}) copy-start(bf16[2048]{0:T(1024)(128)(2,1)} %param.27) | copy-start | bytes 12292
  469.2 254.4 %all-gather.5.cloned.1.call-start = ((), (), s32[]{:S(2)}) async-start(), calls=%async_computation.4 | async-start | bytes 12255232 | tf_op jit(solution)/shard_map/all_gather | solution.py:158
  490.0 37.3 %collective-permute-start.13 = (bf16[128,5632]{1,0:T(8,128)(2,1)}, bf16[128,5632]{1,0:T(8,128)(2,1)S(1)}, u32[]{:S(2)}, u32[]{:S(2)}) collective-permute-start(bf16[128,5632]{1,0:T(8,128)(2,1)} %collective-permute-done.12), channel_id=1, source_target_pairs={{0,2},{2,4},{4,6},{6,8},{8,10},{10,12},{12,14},{14,16},{16,18},{18... | collective-permute-start | bytes 4325384 | tf_op jit(solution)/shard_map/ppermute | solution.py:18
  490.1 247.4 %reduce-scatter.5.cloned.1.call-start = ((), (), s32[]{:S(2)}) async-start(), calls=%async_computation.5 | async-start | bytes 786432 | tf_op jit(solution)/shard_map/reduce_scatter | solution.py:160
  527.3 38.4 %copy-start.21 = (bf16[128,5632]{1,0:T(8,128)(2,1)}, bf16[128,5632]{1,0:T(8,128)(2,1)S(1)}, u32[]{:S(2)}) copy-start(bf16[128,5632]{1,0:T(8,128)(2,1)S(1)} %collective-permute-done.13) | copy-start | bytes 4325380
  527.3 33.4 %collective-permute-start.14 = (bf16[128,5632]{1,0:T(8,128)(2,1)S(1)}, bf16[128,5632]{1,0:T(8,128)(2,1)S(1)}, u32[]{:S(2)}, u32[]{:S(2)}) collective-permute-start(bf16[128,5632]{1,0:T(8,128)(2,1)S(1)} %collective-permute-done.13), channel_id=1, source_target_pairs={{0,2},{2,4},{4,6},{6,8},{8,10},{10,12},{12,14},{14,16},{16,18},{18... | collective-permute-start | bytes 4325384 | tf_op jit(solution)/shard_map/ppermute | solution.py:18
  530.9 34.8 %copy-start.23 = (bf16[64,2048]{1,0:T(8,128)(2,1)}, bf16[64,2048]{1,0:T(8,128)(2,1)S(1)}, u32[]{:S(2)}) copy-start(bf16[64,2048]{1,0:T(8,128)(2,1)S(1)} %fusion.33) | copy-start | bytes 786436
  565.7 8.3 %copy-start.20 = (bf16[128,5632]{1,0:T(8,128)(2,1)S(1)}, bf16[128,5632]{1,0:T(8,128)(2,1)}, u32[]{:S(2)}) copy-start(bf16[128,5632]{1,0:T(8,128)(2,1)} %copy-done.19) | copy-start | bytes 4325380
  568.4 6.8 copy-start.18
  571.2 5.2 copy-start.16
  574.0 3.7 copy-start.14
  575.2 3.7 copy-start.12
  576.4 3.7 copy-start.10
  577.7 3.6 copy-start.8
  578.8 3.7 copy-start.6
  581.3 3.6 copy-start.3
  582.5 3.3 copy-start.4
  583.7 4.3 copy-start.22
  623.2 3.0 collective-permute-start.15
  624.5 6.3 collective-permute-start.16
  633.6 97.8 %copy-start.27 = (bf16[2048]{0:T(1024)(128)(2,1)S(1)}, bf16[2048]{0:T(1024)(128)(2,1)}, u32[]{:S(2)}) copy-start(bf16[2048]{0:T(1024)(128)(2,1)} %param.28) | copy-start | bytes 12292
  633.6 105.0 %copy-start.24 = (bf16[64,2048]{1,0:T(8,128)(2,1)S(1)}, bf16[64,2048]{1,0:T(8,128)(2,1)}, u32[]{:S(2)}) copy-start(bf16[64,2048]{1,0:T(8,128)(2,1)} %copy-done.23) | copy-start | bytes 786436
  723.6 16.8 %copy-start.1 = (bf16[512,2048]{1,0:T(8,128)(2,1)S(1)}, bf16[512,2048]{1,0:T(8,128)(2,1)}, u32[]{:S(2)}) copy-start(bf16[512,2048]{1,0:T(8,128)(2,1)} %param.25) | copy-start | bytes 6291460
Sparse Core Ops, SparseCore 0:
  357.6 92.2 all-gather.2
  469.3 7.0 reduce-scatter.2
  490.2 233.3 all-gather.4
  731.6 5.8 reduce-scatter.4
